TPU v7x, 32 devices: a whole 2x2x4 slice. The times are simulated.
32 devices in a mesh: pp: 4 (over y, x), tp: 8 (over z, core).
Axes of the slice: x: 2, y: 2, z: 4, core: 2. Of those that a mesh axis runs over, the one named last changes fastest.
Arguments:
- entry_stream_rows: bfloat16 [256, 2048], P('pp', 'tp'), may hold values from -21 to 21
- layer_rescale_factor: float32 [4, 2048], P('pp'), may hold values from 0.1 to 1.9
- probe_projection: bfloat16 [4, 2048, 2048], P('pp', 'tp'), may hold values from -0.125 to 0.125
- retention_projection: bfloat16 [4, 2048, 2048], P('pp', 'tp'), may hold values from -0.125 to 0.125
- candidate_projection: bfloat16 [4, 2048, 2048], P('pp', 'tp'), may hold values from -0.125 to 0.125
- emission_filter_matrix: bfloat16 [4, 2048, 2048], P('pp', 'tp'), may hold values from -0.125 to 0.125
- retention_minimum: float32 [4, 2048], P('pp', 'tp'), may hold values from 0.88 to 0.9921875
- decay_spike: float32 [4, 128, 32], P('pp', None, 'tp'), may hold values from -2.1 to 0
- per_group_scale: float32 [4, 64], P('pp'), may hold values from 0.1 to 1.9
Outputs:
- outputs: bfloat16 [256, 2048], P('pp', 'tp')
All inputs are finite; a program needn't handle non-finite values.
Results may differ from a plain program's by a relative error of at most 0.03.
Values may be sent and summed in bfloat16 or wider, within the bound.
A program may use at most 64 MiB of HBM per device.

v0:
```python
import functools

import jax
import jax.numpy as jnp
from jax import lax
from jax.experimental import pallas as pl
from jax.experimental.pallas import tpu as pltpu
from jax.sharding import PartitionSpec as P

HEAD = 64
TILE = 256
EPSILON = 1e-06
F32 = jnp.float32
BF16 = jnp.bfloat16
NT = (((1,), (1,)), ((), ()))
NN = (((1,), (0,)), ((), ()))
TN = (((0,), (0,)), ((), ()))


def mm(a, b, dims):
    return lax.dot_general(a, b, dims, preferred_element_type=F32)


def sigmoid(v):
    return 1.0 / (1.0 + jnp.exp(-v))


def signal_to(semaphore, stage, lane):
    pl.semaphore_signal(
        semaphore,
        inc=1,
        device_id={"pp": stage, "tp": lane},
        device_id_type=pl.DeviceIdType.MESH,
    )


def kernel(
    stages,
    lanes_axis,
    x_ref,
    gain_ref,
    wq_ref,
    wf_ref,
    wi_ref,
    wg_ref,
    low_ref,
    spike_ref,
    scale_ref,
    out_ref,
    weights,
    turned,
    buf,
    res,
    spikes,
    state,
    w_sem,
    in_send,
    direct_sem,
    forward_sem,
    send_sem,
    forward_send,
    out_sem,
):
    rows, cols = x_ref.shape
    heads = cols // HEAD
    width = gain_ref.shape[1]
    chips = lanes_axis // 2
    chunks = stages
    stage = lax.axis_index("pp")
    lane = lax.axis_index("tp")
    core = lax.rem(lane, 2)
    z = lane // 2
    partner = z * 2 + (1 - core)

    loads = []
    for role, ref in enumerate((wq_ref, wf_ref, wi_ref, wg_ref)):
        load = pltpu.make_async_copy(
            ref.at[0], weights.at[pl.ds(role * cols, cols)], w_sem.at[role]
        )
        load.start()
        loads.append(load)

    barrier = pltpu.get_barrier_semaphore()
    for up in range(stages):
        for over in range(chips):
            if up or over:
                signal_to(
                    barrier,
                    lax.rem(stage + up, stages),
                    lax.rem(z + over, chips) * 2 + core,
                )
    signal_to(barrier, stage, partner)
    pl.semaphore_wait(barrier, stages * chips)

    def farthest_first(send):
        for far in range(chips - 1, 0, -1):

            @pl.when(z + far < chips)
            def _():
                send(z + far)

            @pl.when(z - far >= 0)
            def _():
                send(z - far)

    def to_first(target):
        return pltpu.make_async_remote_copy(
            src_ref=x_ref,
            dst_ref=buf.at[stage, core, z],
            send_sem=in_send.at[target],
            recv_sem=direct_sem.at[stage],
            device_id={"pp": 0, "tp": target * 2 + core},
            device_id_type=pl.DeviceIdType.MESH,
        )

    farthest_first(lambda target: to_first(target).start())

    @pl.when(stage != 0)
    def _():
        to_first(z).start()

    @pl.when(stage == 0)
    def _():
        pltpu.make_async_copy(x_ref, buf.at[stage, core, z], direct_sem.at[stage]).start()

    head_of_lane = lax.broadcasted_iota(jnp.int32, (rows, cols), 1) // HEAD
    for part in range(2):
        piece = spike_ref[0, :, part * rows : (part + 1) * rows].T
        wide = jnp.zeros((rows, cols), F32)
        for h in range(heads):
            wide = jnp.where(head_of_lane == h, piece[:, h : h + 1], wide)
        spikes[part] = wide

    tri_row = lax.broadcasted_iota(jnp.int32, (rows, rows), 0)
    tri_col = lax.broadcasted_iota(jnp.int32, (rows, rows), 1)
    tril = tri_row >= tri_col
    tril_ones = jnp.where(tril, 1.0, 0.0).astype(BF16)
    tall_row = lax.rem(lax.broadcasted_iota(jnp.int32, (heads * rows, rows), 0), rows)
    tall_col = lax.broadcasted_iota(jnp.int32, (heads * rows, rows), 1)
    tall_mask = tall_row >= tall_col
    sq_row = lax.broadcasted_iota(jnp.int32, (cols, cols), 0) // HEAD
    sq_col = lax.broadcasted_iota(jnp.int32, (cols, cols), 1) // HEAD
    same_head = sq_row == sq_col
    mean_ones = jnp.where(same_head, 1.0 / HEAD, 0.0).astype(BF16)
    keep_span = 1.0 - low_ref[...]
    out_gain = jnp.concatenate([scale_ref[...]] * heads, axis=1)

    for role, load in enumerate(loads):
        load.wait()

        def turn(k, carry, role=role):
            tile = pl.ds(pl.multiple_of(k * TILE, TILE), TILE)
            turned[tile, role * cols : (role + 1) * cols] = weights[
                role * cols : (role + 1) * cols, tile
            ].T
            return carry

        lax.fori_loop(0, width // TILE, turn, 0)

    def whole_wait(c, which, sem):
        half = buf.at[c, which]
        pltpu.make_async_copy(half, half, sem).wait()

    def forward(c):
        half = buf.at[c, core]
        return pltpu.make_async_remote_copy(
            src_ref=half,
            dst_ref=half,
            send_sem=forward_send.at[c],
            recv_sem=forward_sem.at[c],
            device_id={"pp": stage, "tp": partner},
            device_id_type=pl.DeviceIdType.MESH,
        )

    def to_next(c, target):
        return pltpu.make_async_remote_copy(
            src_ref=res.at[c],
            dst_ref=buf.at[c, core, z],
            send_sem=send_sem.at[c],
            recv_sem=direct_sem.at[c],
            device_id={"pp": lax.rem(stage + 1, stages), "tp": target * 2 + core},
            device_id_type=pl.DeviceIdType.MESH,
        )

    def to_out(c):
        return pltpu.make_async_remote_copy(
            src_ref=res.at[c],
            dst_ref=out_ref,
            send_sem=send_sem.at[c],
            recv_sem=out_sem,
            device_id={"pp": c, "tp": lane},
            device_id_type=pl.DeviceIdType.MESH,
        )

    def step(c, carry):
        whole_wait(c, core, direct_sem.at[c])
        forward(c).start()

        whole_wait(c, 1 - core, forward_sem.at[c])
        current = jnp.concatenate(
            [buf[c, k % 2, k // 2] for k in range(lanes_axis)], axis=1
        ).astype(F32)
        squares = jnp.sum(current * current, axis=1, keepdims=True)
        scaled = (current * gain_ref[...]).astype(BF16)
        product = mm(scaled, turned[...], NN)
        projected = product * lax.rsqrt(squares / width + EPSILON)
        query_pre = projected[:, 0 * cols : 1 * cols]
        forget_pre = projected[:, 1 * cols : 2 * cols]
        values = projected[:, 2 * cols : 3 * cols].astype(BF16)
        gate_pre = projected[:, 3 * cols : 4 * cols]

        key_in = keep_span * sigmoid(-forget_pre)
        log_forget = jnp.log(1.0 - key_in) + spikes[lax.rem(c, 2)]
        high = log_forget.astype(BF16)
        low = (log_forget - high.astype(F32)).astype(BF16)
        running = mm(tril_ones, high, NN) + mm(tril_ones, low, NN)
        ending = running[rows - 1 : rows, :]
        query_scaled = query_pre * sigmoid(query_pre) * jnp.exp(running)
        key_scaled = (key_in * jnp.exp(-running)).astype(BF16)
        key_end = (key_in * jnp.exp(ending - running)).astype(BF16)
        query_bf = query_scaled.astype(BF16)
        tall_query = jnp.concatenate(
            [jnp.where(head_of_lane == h, query_scaled, 0.0).astype(BF16) for h in range(heads)],
            axis=0,
        )
        scores = jnp.where(tall_mask, mm(tall_query, key_scaled, NT), 0.0).astype(BF16)
        tall_mixed = mm(scores, values, NN)
        memory = jnp.where(lax.rem(c, 2) == 0, 0.0, state[...])
        mixed = mm(query_bf, memory.astype(BF16), NT)
        inner = tall_mixed[0:rows]
        for h in range(1, heads):
            inner = jnp.where(head_of_lane == h, tall_mixed[h * rows : (h + 1) * rows], inner)
        mixed = mixed + inner
        mean_square = mm((mixed * mixed).astype(BF16), mean_ones, NN)
        branch = mixed * lax.rsqrt(mean_square + EPSILON) * out_gain
        branch = branch * (gate_pre * sigmoid(gate_pre))
        res[c] = (buf[c, core, z].astype(F32) + branch).astype(BF16)

        @pl.when(stage != stages - 1)
        def _():
            farthest_first(lambda target: to_next(c, target).start())
            to_next(c, z).start()

        @pl.when((stage == stages - 1) & (c != stage))
        def _():
            to_out(c).start()

        @pl.when((stage == stages - 1) & (c == stage))
        def _():
            pltpu.make_async_copy(res.at[c], out_ref, out_sem).start()

        added = jnp.where(same_head, mm(values, key_end, TN), 0.0)
        state[...] = memory * jnp.exp(ending) + added
        return carry

    lax.fori_loop(0, chunks, step, 0)

    farthest_first(lambda target: to_first(target).wait_send())

    @pl.when(stage != 0)
    def _():
        to_first(z).wait_send()

    def drain(c, carry):
        forward(c).wait_send()

        @pl.when(stage != stages - 1)
        def _():
            whole_wait(c, core, send_sem.at[c])

        @pl.when((stage == stages - 1) & (c != stage))
        def _():
            to_out(c).wait_send()

        return carry

    lax.fori_loop(0, chunks, drain, 0)
    pltpu.make_async_copy(out_ref, out_ref, out_sem).wait()


def solution(mesh):
    stages = mesh.shape["pp"]
    lanes_axis = mesh.shape["tp"]
    chips = lanes_axis // 2

    def step(x, gain, wq, wf, wi, wg, low, spike, scale):
        rows, cols = x.shape
        width = gain.shape[1]
        vmem = pl.BlockSpec(memory_space=pltpu.VMEM)
        hbm = pl.BlockSpec(memory_space=pl.ANY)
        dma = pltpu.SemaphoreType.DMA
        return pl.pallas_call(
            functools.partial(kernel, stages, lanes_axis),
            out_shape=jax.ShapeDtypeStruct((rows, cols), BF16),
            in_specs=[vmem, vmem, hbm, hbm, hbm, hbm, vmem, vmem, vmem],
            out_specs=vmem,
            scratch_shapes=[
                pltpu.VMEM((4 * cols, width), BF16),
                pltpu.VMEM((width, 4 * cols), BF16),
                pltpu.VMEM((stages, 2, chips, rows, cols), BF16),
                pltpu.VMEM((stages, rows, cols), BF16),
                pltpu.VMEM((2, rows, cols), F32),
                pltpu.VMEM((cols, cols), F32),
                dma((4,)),
                dma((chips,)),
                dma((stages,)),
                dma((stages,)),
                dma((stages,)),
                dma((stages,)),
                dma,
            ],
            compiler_params=pltpu.CompilerParams(
                collective_id=0, has_side_effects=True, vmem_limit_bytes=67043328
            ),
        )(x, gain, wq, wf, wi, wg, low, spike.transpose(0, 2, 1), scale)

    in_specs = (
        P("pp", "tp"),
        P("pp", None),
        P("pp", "tp", None),
        P("pp", "tp", None),
        P("pp", "tp", None),
        P("pp", "tp", None),
        P("pp", "tp"),
        P("pp", None, "tp"),
        P("pp", None),
    )
    return jax.shard_map(
        step, mesh=mesh, in_specs=in_specs, out_specs=P("pp", "tp"), check_vma=False
    )
```

profile of v0, /device:TPU:7, one launch (start us, length us, event | category | flops | bytes accessed | tf_op | source)
XLA Modules:
  0.0 46.6 jit_solution(1681539567043064044)
XLA Ops:
  0.0 45.2 %shard_map.91 = bf16[64,256]{1,0:T(8,128)(2,1)} custom-call(bf16[64,256]{1,0:T(8,128)(2,1)} %x_ref.1, f32[1,2048]{1,0:T(1,128)} %gain_ref.1, bf16[1,256,2048]{2,1,0:T(8,128)(2,1)} %wq_ref.1, bf16[1,256,2048]{2,1,0:T(8,128)(2,1)} %wf_ref.1, bf16[1,256,2048]{2,1,0:T(8,128)(2,1)} %wi_ref.1, bf16[1,256,2048]{2,1,0:T(8,128)(2,1)} %wg_ref.1, f32[1,256]{1,0:T(1,128)} %low_ref.1, ...), custom_call_target="tpu_custom_call" | custom-call | tf_op jit(solution)/shard_map/pallas_call | solution.py:292
  45.2 1.4 %copy.11 = bf16[64,256]{1,0:T(8,128)(2,1)} copy(bf16[64,256]{1,0:T(8,128)(2,1)} %shard_map.91) | data formatting | bytes 65536
where the time goes:
time: 46.9 us; the launch traced here: 46.6 us
  Pallas kernels  45.2 us (96%)
  local copies, waits for them, and re-layouts  1.38 us (3%)
    pallas_call x1, Pallas kernels, step(): pl.pallas_call(functools.partial(kernel, stages, lanes_axis), out_shape=j...  45.2 us
    unnamed x1, local copies, waits for them, and re-layouts  1.38 us

commit v1 on v0

v1 whole, which is shorter than its diff:
```python
import functools

import jax
import jax.numpy as jnp
from jax import lax
from jax.experimental import pallas as pl
from jax.experimental.pallas import tpu as pltpu
from jax.sharding import PartitionSpec as P

HEAD = 64
TILE = 256
EPSILON = 1e-06
F32 = jnp.float32
BF16 = jnp.bfloat16
NT = (((1,), (1,)), ((), ()))
NN = (((1,), (0,)), ((), ()))
TN = (((0,), (0,)), ((), ()))


def mm(a, b, dims):
    return lax.dot_general(a, b, dims, preferred_element_type=F32)


def sigmoid(v):
    return 1.0 / (1.0 + jnp.exp(-v))


def at(stage, lane):
    return {"pp": stage, "tp": lane}


def kernel(
    stages,
    lanes_axis,
    x_ref,
    gain_ref,
    wq_ref,
    wf_ref,
    wi_ref,
    wg_ref,
    low_ref,
    spike_ref,
    scale_ref,
    out_ref,
    xv,
    gain_v,
    scale_v,
    lows,
    spike_raw,
    weights,
    turned,
    buf,
    res,
    spikes,
    state,
    outv,
    load_sem,
    w_sem,
    swap_send,
    swap_recv,
    in_send,
    direct_sem,
    forward_sem,
    forward_send,
    send_sem,
    out_sem,
):
    rows, cols = xv.shape
    size = buf.shape[4]
    heads = cols // HEAD
    width = gain_v.shape[1]
    positions = spike_raw.shape[2]
    parts = positions // size
    spans = positions // rows
    chips = lanes_axis // 2
    slots = stages
    last = stages - 1
    stage = lax.axis_index("pp")
    lane = lax.axis_index("tp")
    core = lax.rem(lane, 2)
    other = 1 - core
    z = lane // 2
    partner = z * 2 + other

    barrier = pltpu.get_barrier_semaphore()
    for up in range(stages):
        for over in range(lanes_axis):
            if up or over:
                pl.semaphore_signal(
                    barrier,
                    inc=1,
                    device_id=at(
                        lax.rem(stage + up, stages), lax.rem(lane + over, lanes_axis)
                    ),
                    device_id_type=pl.DeviceIdType.MESH,
                )

    small = [
        pltpu.make_async_copy(gain_ref, gain_v, load_sem.at[1]),
        pltpu.make_async_copy(scale_ref, scale_v, load_sem.at[2]),
        pltpu.make_async_copy(low_ref, lows.at[core], load_sem.at[3]),
        pltpu.make_async_copy(spike_ref.at[0], spike_raw.at[core], load_sem.at[4]),
    ]
    x_load = pltpu.make_async_copy(x_ref, xv, load_sem.at[0])
    x_load.start()
    for load in small:
        load.start()
    loads = []
    for role, ref in enumerate((wq_ref, wf_ref, wi_ref, wg_ref)):
        load = pltpu.make_async_copy(
            ref.at[0], weights.at[pl.ds(role * cols, cols)], w_sem.at[role]
        )
        load.start()
        loads.append(load)

    sequence = stage // spans
    in_parity = lax.rem(sequence, 2)
    in_slot = (sequence // 2) * parts + lax.rem(stage, spans) * 2

    def farthest_first(send):
        for far in range(chips - 1, 0, -1):

            @pl.when(z + far < chips)
            def _():
                send(z + far)

            @pl.when(z - far >= 0)
            def _():
                send(z - far)

    def to_first(target, half):
        return pltpu.make_async_remote_copy(
            src_ref=xv.at[pl.ds(half * size, size)],
            dst_ref=buf.at[in_parity, in_slot + half, core, z],
            send_sem=in_send.at[target],
            recv_sem=direct_sem.at[in_parity, in_slot + half],
            device_id=at(0, target * 2 + core),
            device_id_type=pl.DeviceIdType.MESH,
        )

    def enter():
        for half in range(2):
            farthest_first(lambda target: to_first(target, half).start())

            @pl.when(stage != 0)
            def _():
                to_first(z, half).start()

            @pl.when(stage == 0)
            def _():
                pltpu.make_async_copy(
                    x_ref.at[pl.ds(half * size, size)],
                    buf.at[in_parity, in_slot + half, core, z],
                    direct_sem.at[in_parity, in_slot + half],
                ).start()

    def swap_small(which):
        src, dst = (
            (lows.at[core], lows.at[core])
            if which == 0
            else (spike_raw.at[core], spike_raw.at[core])
        )
        return pltpu.make_async_remote_copy(
            src_ref=src,
            dst_ref=dst,
            send_sem=swap_send.at[1 + which],
            recv_sem=swap_recv.at[1 + which],
            device_id=at(stage, partner),
            device_id_type=pl.DeviceIdType.MESH,
        )

    def swap_tile(k):
        tile = turned.at[core, pl.ds(pl.multiple_of(k * TILE, TILE), TILE)]
        return pltpu.make_async_remote_copy(
            src_ref=tile,
            dst_ref=tile,
            send_sem=swap_send.at[0],
            recv_sem=swap_recv.at[0],
            device_id=at(stage, partner),
            device_id_type=pl.DeviceIdType.MESH,
        )

    head_of_lane = lax.broadcasted_iota(jnp.int32, (size, cols), 1) // HEAD
    tri_row = lax.broadcasted_iota(jnp.int32, (size, size), 0)
    tri_col = lax.broadcasted_iota(jnp.int32, (size, size), 1)
    tril_ones = jnp.where(tri_row >= tri_col, 1.0, 0.0).astype(BF16)
    tall_row = lax.rem(lax.broadcasted_iota(jnp.int32, (heads * size, size), 0), size)
    tall_col = lax.broadcasted_iota(jnp.int32, (heads * size, size), 1)
    tall_mask = tall_row >= tall_col
    sq_row = lax.broadcasted_iota(jnp.int32, (cols, cols), 0) // HEAD
    sq_col = lax.broadcasted_iota(jnp.int32, (cols, cols), 1) // HEAD
    same_head = sq_row == sq_col
    mean_ones = jnp.where(same_head, 1.0 / HEAD, 0.0).astype(BF16)

    def spread(half):
        for part in range(parts):
            piece = spike_raw[half, :, part * size : (part + 1) * size].T
            wide = jnp.zeros((size, cols), F32)
            for h in range(heads):
                wide = jnp.where(head_of_lane == h, piece[:, h : h + 1], wide)
            spikes[half, part] = wide

    for load in small:
        load.wait()
    x_load.wait()
    spread(core)

    pl.semaphore_wait(barrier, stages * lanes_axis - 1)

    @pl.when(in_slot == 0)
    def _():
        enter()

    @pl.when(stage != 0)
    def _():
        swap_small(0).start()
        swap_small(1).start()

    for load in loads:
        load.wait()

    def turn(k, carry):
        tile = pl.ds(pl.multiple_of(k * TILE, TILE), TILE)
        for role in range(4):
            turned[core, tile, role * cols : (role + 1) * cols] = weights[
                role * cols : (role + 1) * cols, tile
            ].T

        @pl.when((stage != 0) & (k > 0))
        def _():
            swap_tile(k - 1).start()

        return carry

    lax.fori_loop(0, width // TILE, turn, 0)

    @pl.when(in_slot != 0)
    def _():
        enter()

    def whole_wait(ref, sem):
        pltpu.make_async_copy(ref, ref, sem).wait()

    def gather(parity, slot):
        current = jnp.concatenate(
            [buf[parity, slot, k % 2, k // 2] for k in range(lanes_axis)], axis=1
        ).astype(F32)
        squares = jnp.sum(current * current, axis=1, keepdims=True)
        scaled = (current * gain_v[...]).astype(BF16)
        return scaled, lax.rsqrt(squares / width + EPSILON)

    out_gain = jnp.concatenate([scale_v[...]] * heads, axis=1)

    def mix(product, inverse, half, part, memory, stream):
        projected = product * inverse
        query_pre = projected[:, 0 * cols : 1 * cols]
        forget_pre = projected[:, 1 * cols : 2 * cols]
        values = projected[:, 2 * cols : 3 * cols].astype(BF16)
        gate_pre = projected[:, 3 * cols : 4 * cols]

        key_in = (1.0 - lows[half]) * sigmoid(-forget_pre)
        log_forget = jnp.log(1.0 - key_in) + spikes[half, part]
        high = log_forget.astype(BF16)
        low = (log_forget - high.astype(F32)).astype(BF16)
        running = mm(tril_ones, high, NN) + mm(tril_ones, low, NN)
        ending = running[size - 1 : size, :]
        query_scaled = query_pre * sigmoid(query_pre) * jnp.exp(running)
        key_scaled = (key_in * jnp.exp(-running)).astype(BF16)
        key_end = (key_in * jnp.exp(ending - running)).astype(BF16)
        query_bf = query_scaled.astype(BF16)
        tall_query = jnp.concatenate(
            [jnp.where(head_of_lane == h, query_scaled, 0.0).astype(BF16) for h in range(heads)],
            axis=0,
        )
        scores = jnp.where(tall_mask, mm(tall_query, key_scaled, NT), 0.0).astype(BF16)
        tall_mixed = mm(scores, values, NN)
        mixed = mm(query_bf, memory.astype(BF16), NT)
        inner = tall_mixed[0:size]
        for h in range(1, heads):
            inner = jnp.where(head_of_lane == h, tall_mixed[h * size : (h + 1) * size], inner)
        mixed = mixed + inner
        mean_square = mm((mixed * mixed).astype(BF16), mean_ones, NN)
        branch = mixed * lax.rsqrt(mean_square + EPSILON) * out_gain
        branch = branch * (gate_pre * sigmoid(gate_pre))
        return (stream + branch).astype(BF16), (values, key_end, ending)

    def advance(memory, carried):
        values, key_end, ending = carried
        added = jnp.where(same_head, mm(values, key_end, TN), 0.0)
        return memory * jnp.exp(ending) + added

    def to_next(slot, index, parity, half, target, to_core):
        return pltpu.make_async_remote_copy(
            src_ref=res.at[slot, index],
            dst_ref=buf.at[parity, slot, half, z],
            send_sem=send_sem.at[slot, index],
            recv_sem=direct_sem.at[parity, slot],
            device_id=at(lax.rem(stage + 1, stages), target * 2 + to_core),
            device_id_type=pl.DeviceIdType.MESH,
        )

    def forward(parity, slot):
        half = buf.at[parity, slot, core]
        return pltpu.make_async_remote_copy(
            src_ref=half,
            dst_ref=half,
            send_sem=forward_send.at[parity, slot],
            recv_sem=forward_sem.at[parity, slot],
            device_id=at(stage, partner),
            device_id_type=pl.DeviceIdType.MESH,
        )

    @pl.when(stage == 0)
    def _():
        steps = 2 * slots

        def pass_on(t):
            parity, slot = lax.rem(t, 2), t // 2
            whole_wait(buf.at[parity, slot, core], direct_sem.at[parity, slot])
            forward(parity, slot).start()

        pass_on(0)

        def step(t, carry):
            parity, slot = lax.rem(t, 2), t // 2
            part = lax.rem(slot, parts)
            whole_wait(buf.at[parity, slot, other], forward_sem.at[parity, slot])
            scaled, inverse = gather(parity, slot)
            product = mm(scaled, turned[core], NN)

            @pl.when(t + 1 < steps)
            def _():
                pass_on(t + 1)

            memory = jnp.where(part == 0, 0.0, state[parity])
            stream = buf[parity, slot, core, z].astype(F32)
            result, carried = mix(product, inverse, core, part, memory, stream)
            res[slot, parity] = result
            to_core = 1 - parity
            farthest_first(
                lambda target: to_next(slot, parity, parity, core, target, to_core).start()
            )
            to_next(slot, parity, parity, core, z, to_core).start()
            state[parity] = advance(memory, carried)
            return carry

        lax.fori_loop(0, steps, step, 0)

        def drain(t, carry):
            parity, slot = lax.rem(t, 2), t // 2
            forward(parity, slot).wait_send()
            whole_wait(buf.at[parity, slot, core], send_sem.at[slot, parity])
            return carry

        lax.fori_loop(0, steps, drain, 0)

    @pl.when(stage != 0)
    def _():
        tiles = width // TILE
        swap_tile(tiles - 1).start()
        swap_small(0).wait_recv()
        swap_small(1).wait_recv()
        spread(other)
        whole_wait(turned.at[other], swap_recv.at[0])
        parity = lax.rem(core + stage, 2)

        def to_out(slot, half):
            part = lax.rem(slot, parts)
            where = ((slot // parts) * 2 + parity) * spans + part // 2
            return where, lax.rem(part, 2)

        def out_copy(slot, half):
            where, low_high = to_out(slot, half)
            return pltpu.make_async_remote_copy(
                src_ref=res.at[slot, half],
                dst_ref=outv.at[low_high],
                send_sem=send_sem.at[slot, half],
                recv_sem=out_sem,
                device_id=at(where, z * 2 + half),
                device_id_type=pl.DeviceIdType.MESH,
            )

        def stays(slot, half):
            where, _ = to_out(slot, half)
            return (where == stage) & (core == half)

        def step(slot, carry):
            part = lax.rem(slot, parts)
            whole_wait(buf.at[parity, slot], direct_sem.at[parity, slot])
            scaled, inverse = gather(parity, slot)
            kept = []
            for half in range(2):
                product = mm(scaled, turned[half], NN)
                memory = jnp.where(part == 0, 0.0, state[half])
                stream = buf[parity, slot, half, z].astype(F32)
                result, carried = mix(product, inverse, half, part, memory, stream)
                res[slot, half] = result
                kept.append((memory, carried))

            @pl.when(stage != last)
            def _():
                for half in range(2):
                    farthest_first(
                        lambda target: to_next(
                            slot, half, parity, half, target, other
                        ).start()
                    )
                    to_next(slot, half, parity, half, z, other).start()

            for half in range(2):

                @pl.when((stage == last) & ~stays(slot, half))
                def _():
                    out_copy(slot, half).start()

                @pl.when((stage == last) & stays(slot, half))
                def _():
                    _, low_high = to_out(slot, half)
                    pltpu.make_async_copy(
                        res.at[slot, half], outv.at[low_high], out_sem
                    ).start()

            for half in range(2):
                memory, carried = kept[half]
                state[half] = advance(memory, carried)
            return carry

        lax.fori_loop(0, slots, step, 0)

        def drain(slot, carry):
            for half in range(2):

                @pl.when(stage != last)
                def _():
                    whole_wait(buf.at[0, 0, 0], send_sem.at[slot, half])

                @pl.when((stage == last) & ~stays(slot, half))
                def _():
                    out_copy(slot, half).wait_send()

            return carry

        lax.fori_loop(0, slots, drain, 0)
        whole_wait(turned.at[core], swap_send.at[0])
        swap_small(0).wait_send()
        swap_small(1).wait_send()

    for target in range(chips):

        @pl.when((stage != 0) | (z != target))
        def _():
            whole_wait(xv, in_send.at[target])

    whole_wait(outv, out_sem)
    for half in range(2):
        out_ref[half * size : (half + 1) * size] = outv[half]


def solution(mesh):
    stages = mesh.shape["pp"]
    lanes_axis = mesh.shape["tp"]
    chips = lanes_axis // 2

    def step(x, gain, wq, wf, wi, wg, low, spike, scale):
        rows, cols = x.shape
        width = gain.shape[1]
        positions = spike.shape[1]
        heads = cols // HEAD
        size = rows // 2
        parts = positions // size
        vmem = pl.BlockSpec(memory_space=pltpu.VMEM)
        hbm = pl.BlockSpec(memory_space=pl.ANY)
        dma = pltpu.SemaphoreType.DMA
        return pl.pallas_call(
            functools.partial(kernel, stages, lanes_axis),
            out_shape=jax.ShapeDtypeStruct((rows, cols), BF16),
            in_specs=[hbm] * 9,
            out_specs=vmem,
            scratch_shapes=[
                pltpu.VMEM((rows, cols), BF16),
                pltpu.VMEM((1, width), F32),
                pltpu.VMEM(scale.shape, F32),
                pltpu.VMEM((2, 1, cols), F32),
                pltpu.VMEM((2, heads, positions), F32),
                pltpu.VMEM((4 * cols, width), BF16),
                pltpu.VMEM((2, width, 4 * cols), BF16),
                pltpu.VMEM((2, stages, 2, chips, size, cols), BF16),
                pltpu.VMEM((stages, 2, size, cols), BF16),
                pltpu.VMEM((2, parts, size, cols), F32),
                pltpu.VMEM((2, cols, cols), F32),
                pltpu.VMEM((2, size, cols), BF16),
                dma((5,)),
                dma((4,)),
                dma((3,)),
                dma((3,)),
                dma((chips,)),
                dma((2, stages)),
                dma((2, stages)),
                dma((2, stages)),
                dma((stages, 2)),
                dma,
            ],
            compiler_params=pltpu.CompilerParams(
                collective_id=0, has_side_effects=True, vmem_limit_bytes=67043328
            ),
        )(x, gain, wq, wf, wi, wg, low, spike.transpose(0, 2, 1), scale)

    in_specs = (
        P("pp", "tp"),
        P("pp", None),
        P("pp", "tp", None),
        P("pp", "tp", None),
        P("pp", "tp", None),
        P("pp", "tp", None),
        P("pp", "tp"),
        P("pp", None, "tp"),
        P("pp", None),
    )
    return jax.shard_map(
        step, mesh=mesh, in_specs=in_specs, out_specs=P("pp", "tp"), check_vma=False
    )
```

time: 46.9 us -> 49.1 us (1.047)
  the two profiles are of different devices: /device:TPU:7 before, /device:TPU:3 now
where the time goes in v1:
time: 49.1 us; the launch traced here: 49 us
  Pallas kernels  47.6 us (97%)
  local copies, waits for them, and re-layouts  1.38 us (3%)
    pallas_call x1, Pallas kernels, step(): pl.pallas_call(functools.partial(kernel, stages, lanes_axis), out_shape=j...  47.6 us
    unnamed x1, local copies, waits for them, and re-layouts  1.38 us

profile of v1, /device:TPU:3, one launch (start us, length us, event | category | flops | bytes accessed | tf_op | source)
XLA Modules:
  0.0 49.0 jit_solution(565109691940692767)
XLA Ops:
  0.0 47.6 %shard_map.91 = bf16[64,256]{1,0:T(8,128)(2,1)} custom-call(bf16[64,256]{1,0:T(8,128)(2,1)} %x_ref.1, f32[1,2048]{1,0:T(1,128)} %gain_ref.1, bf16[1,256,2048]{2,1,0:T(8,128)(2,1)} %wq_ref.1, bf16[1,256,2048]{2,1,0:T(8,128)(2,1)} %wf_ref.1, bf16[1,256,2048]{2,1,0:T(8,128)(2,1)} %wi_ref.1, bf16[1,256,2048]{2,1,0:T(8,128)(2,1)} %wg_ref.1, f32[1,256]{1,0:T(1,128)} %low_ref.1, ...), custom_call_target="tpu_custom_call" | custom-call | tf_op jit(solution)/shard_map/pallas_call | solution.py:474
  47.6 1.4 %copy.11 = bf16[64,256]{1,0:T(8,128)(2,1)} copy(bf16[64,256]{1,0:T(8,128)(2,1)} %shard_map.91) | data formatting | bytes 65536

commit v2 on v1

--- a/solution.py
+++ b/solution.py
@@ -10,6 +10,7 @@
 HEAD = 64
 TILE = 256
 EPSILON = 1e-06
+GRANT = 40 * 2**20
 F32 = jnp.float32
 BF16 = jnp.bfloat16
 NT = (((1,), (1,)), ((), ()))
@@ -53,7 +54,6 @@
     res,
     spikes,
     state,
-    outv,
     load_sem,
     w_sem,
     swap_send,
@@ -131,9 +131,9 @@
     def to_first(target, half):
         return pltpu.make_async_remote_copy(
             src_ref=xv.at[pl.ds(half * size, size)],
-            dst_ref=buf.at[in_parity, in_slot + half, core, z],
+            dst_ref=buf.at[in_slot + half, in_parity, core, z],
             send_sem=in_send.at[target],
-            recv_sem=direct_sem.at[in_parity, in_slot + half],
+            recv_sem=direct_sem.at[in_slot + half],
             device_id=at(0, target * 2 + core),
             device_id_type=pl.DeviceIdType.MESH,
         )
@@ -150,8 +150,8 @@
             def _():
                 pltpu.make_async_copy(
                     x_ref.at[pl.ds(half * size, size)],
-                    buf.at[in_parity, in_slot + half, core, z],
-                    direct_sem.at[in_parity, in_slot + half],
+                    buf.at[in_slot + half, in_parity, core, z],
+                    direct_sem.at[in_slot + half],
                 ).start()
 
     def swap_small(which):
@@ -200,22 +200,22 @@
                 wide = jnp.where(head_of_lane == h, piece[:, h : h + 1], wide)
             spikes[half, part] = wide
 
-    for load in small:
-        load.wait()
     x_load.wait()
-    spread(core)
-
     pl.semaphore_wait(barrier, stages * lanes_axis - 1)
 
     @pl.when(in_slot == 0)
     def _():
         enter()
+
+    for load in small:
+        load.wait()
 
     @pl.when(stage != 0)
     def _():
         swap_small(0).start()
         swap_small(1).start()
 
+    spread(core)
     for load in loads:
         load.wait()
 
@@ -241,9 +241,15 @@
     def whole_wait(ref, sem):
         pltpu.make_async_copy(ref, ref, sem).wait()
 
-    def gather(parity, slot):
+    def gather(slot, parities):
         current = jnp.concatenate(
-            [buf[parity, slot, k % 2, k // 2] for k in range(lanes_axis)], axis=1
+            [
+                jnp.concatenate(
+                    [buf[slot, parity, k % 2, k // 2] for k in range(lanes_axis)], axis=1
+                )
+                for parity in parities
+            ],
+            axis=0,
         ).astype(F32)
         squares = jnp.sum(current * current, axis=1, keepdims=True)
         scaled = (current * gain_v[...]).astype(BF16)
@@ -289,70 +295,64 @@
         added = jnp.where(same_head, mm(values, key_end, TN), 0.0)
         return memory * jnp.exp(ending) + added
 
-    def to_next(slot, index, parity, half, target, to_core):
-        return pltpu.make_async_remote_copy(
-            src_ref=res.at[slot, index],
-            dst_ref=buf.at[parity, slot, half, z],
-            send_sem=send_sem.at[slot, index],
-            recv_sem=direct_sem.at[parity, slot],
-            device_id=at(lax.rem(stage + 1, stages), target * 2 + to_core),
-            device_id_type=pl.DeviceIdType.MESH,
-        )
-
-    def forward(parity, slot):
-        half = buf.at[parity, slot, core]
-        return pltpu.make_async_remote_copy(
-            src_ref=half,
-            dst_ref=half,
-            send_sem=forward_send.at[parity, slot],
-            recv_sem=forward_sem.at[parity, slot],
-            device_id=at(stage, partner),
-            device_id_type=pl.DeviceIdType.MESH,
-        )
-
     @pl.when(stage == 0)
     def _():
-        steps = 2 * slots
-
-        def pass_on(t):
-            parity, slot = lax.rem(t, 2), t // 2
-            whole_wait(buf.at[parity, slot, core], direct_sem.at[parity, slot])
-            forward(parity, slot).start()
+        def to_next(slot, parity, target):
+            return pltpu.make_async_remote_copy(
+                src_ref=res.at[slot, parity],
+                dst_ref=buf.at[slot, parity, core, z],
+                send_sem=send_sem.at[slot],
+                recv_sem=direct_sem.at[slot],
+                device_id=at(1, target * 2 + 1 - parity),
+                device_id_type=pl.DeviceIdType.MESH,
+            )
+
+        def forward(slot):
+            half = buf.at[slot, :, core]
+            return pltpu.make_async_remote_copy(
+                src_ref=half,
+                dst_ref=half,
+                send_sem=forward_send.at[slot],
+                recv_sem=forward_sem.at[slot],
+                device_id=at(stage, partner),
+                device_id_type=pl.DeviceIdType.MESH,
+            )
+
+        def pass_on(slot):
+            whole_wait(buf.at[slot, :, core], direct_sem.at[slot])
+            forward(slot).start()
 
         pass_on(0)
 
-        def step(t, carry):
-            parity, slot = lax.rem(t, 2), t // 2
+        def step(slot, carry):
             part = lax.rem(slot, parts)
-            whole_wait(buf.at[parity, slot, other], forward_sem.at[parity, slot])
-            scaled, inverse = gather(parity, slot)
+            whole_wait(buf.at[slot, :, other], forward_sem.at[slot])
+            scaled, inverse = gather(slot, (0, 1))
             product = mm(scaled, turned[core], NN)
 
-            @pl.when(t + 1 < steps)
-            def _():
-                pass_on(t + 1)
-
-            memory = jnp.where(part == 0, 0.0, state[parity])
-            stream = buf[parity, slot, core, z].astype(F32)
-            result, carried = mix(product, inverse, core, part, memory, stream)
-            res[slot, parity] = result
-            to_core = 1 - parity
-            farthest_first(
-                lambda target: to_next(slot, parity, parity, core, target, to_core).start()
-            )
-            to_next(slot, parity, parity, core, z, to_core).start()
-            state[parity] = advance(memory, carried)
+            @pl.when(slot + 1 < slots)
+            def _():
+                pass_on(slot + 1)
+
+            for parity in range(2):
+                own = slice(parity * size, (parity + 1) * size)
+                memory = jnp.where(part == 0, 0.0, state[parity])
+                stream = buf[slot, parity, core, z].astype(F32)
+                result, carried = mix(product[own], inverse[own], core, part, memory, stream)
+                res[slot, parity] = result
+                farthest_first(lambda target: to_next(slot, parity, target).start())
+                to_next(slot, parity, z).start()
+                state[parity] = advance(memory, carried)
             return carry
 
-        lax.fori_loop(0, steps, step, 0)
-
-        def drain(t, carry):
-            parity, slot = lax.rem(t, 2), t // 2
-            forward(parity, slot).wait_send()
-            whole_wait(buf.at[parity, slot, core], send_sem.at[slot, parity])
+        lax.fori_loop(0, slots, step, 0)
+
+        def drain(slot, carry):
+            forward(slot).wait_send()
+            whole_wait(buf.at[slot, 0], send_sem.at[slot])
             return carry
 
-        lax.fori_loop(0, steps, drain, 0)
+        lax.fori_loop(0, slots, drain, 0)
 
     @pl.when(stage != 0)
     def _():
@@ -364,48 +364,54 @@
         whole_wait(turned.at[other], swap_recv.at[0])
         parity = lax.rem(core + stage, 2)
 
-        def to_out(slot, half):
+        def to_next(slot, target):
+            return pltpu.make_async_remote_copy(
+                src_ref=res.at[slot],
+                dst_ref=buf.at[slot, parity, :, z],
+                send_sem=send_sem.at[slot],
+                recv_sem=direct_sem.at[slot],
+                device_id=at(lax.rem(stage + 1, stages), target * 2 + other),
+                device_id_type=pl.DeviceIdType.MESH,
+            )
+
+        def owner(slot):
             part = lax.rem(slot, parts)
-            where = ((slot // parts) * 2 + parity) * spans + part // 2
-            return where, lax.rem(part, 2)
+            return ((slot // parts) * 2 + parity) * spans + part // 2
+
+        def place(slot):
+            start = pl.multiple_of(lax.rem(slot, 2) * size, size)
+            return out_ref.at[pl.ds(start, size)]
 
         def out_copy(slot, half):
-            where, low_high = to_out(slot, half)
             return pltpu.make_async_remote_copy(
                 src_ref=res.at[slot, half],
-                dst_ref=outv.at[low_high],
-                send_sem=send_sem.at[slot, half],
+                dst_ref=place(slot),
+                send_sem=send_sem.at[slot],
                 recv_sem=out_sem,
-                device_id=at(where, z * 2 + half),
+                device_id=at(owner(slot), z * 2 + half),
                 device_id_type=pl.DeviceIdType.MESH,
             )
 
         def stays(slot, half):
-            where, _ = to_out(slot, half)
-            return (where == stage) & (core == half)
+            return (owner(slot) == stage) & (core == half)
 
         def step(slot, carry):
             part = lax.rem(slot, parts)
-            whole_wait(buf.at[parity, slot], direct_sem.at[parity, slot])
-            scaled, inverse = gather(parity, slot)
+            whole_wait(buf.at[slot, parity], direct_sem.at[slot])
+            scaled, inverse = gather(slot, (parity,))
             kept = []
             for half in range(2):
                 product = mm(scaled, turned[half], NN)
                 memory = jnp.where(part == 0, 0.0, state[half])
-                stream = buf[parity, slot, half, z].astype(F32)
+                stream = buf[slot, parity, half, z].astype(F32)
                 result, carried = mix(product, inverse, half, part, memory, stream)
                 res[slot, half] = result
                 kept.append((memory, carried))
 
             @pl.when(stage != last)
             def _():
-                for half in range(2):
-                    farthest_first(
-                        lambda target: to_next(
-                            slot, half, parity, half, target, other
-                        ).start()
-                    )
-                    to_next(slot, half, parity, half, z, other).start()
+                farthest_first(lambda target: to_next(slot, target).start())
+                to_next(slot, z).start()
 
             for half in range(2):
 
@@ -415,10 +421,7 @@
 
                 @pl.when((stage == last) & stays(slot, half))
                 def _():
-                    _, low_high = to_out(slot, half)
-                    pltpu.make_async_copy(
-                        res.at[slot, half], outv.at[low_high], out_sem
-                    ).start()
+                    pltpu.make_async_copy(res.at[slot, half], place(slot), out_sem).start()
 
             for half in range(2):
                 memory, carried = kept[half]
@@ -428,11 +431,11 @@
         lax.fori_loop(0, slots, step, 0)
 
         def drain(slot, carry):
+            @pl.when(stage != last)
+            def _():
+                whole_wait(buf.at[slot, 0], send_sem.at[slot])
+
             for half in range(2):
-
-                @pl.when(stage != last)
-                def _():
-                    whole_wait(buf.at[0, 0, 0], send_sem.at[slot, half])
 
                 @pl.when((stage == last) & ~stays(slot, half))
                 def _():
@@ -451,9 +454,7 @@
         def _():
             whole_wait(xv, in_send.at[target])
 
-    whole_wait(outv, out_sem)
-    for half in range(2):
-        out_ref[half * size : (half + 1) * size] = outv[half]
+    whole_wait(out_ref, out_sem)
 
 
 def solution(mesh):
@@ -484,26 +485,30 @@
                 pltpu.VMEM((2, heads, positions), F32),
                 pltpu.VMEM((4 * cols, width), BF16),
                 pltpu.VMEM((2, width, 4 * cols), BF16),
-                pltpu.VMEM((2, stages, 2, chips, size, cols), BF16),
+                pltpu.VMEM((stages, 2, 2, chips, size, cols), BF16),
                 pltpu.VMEM((stages, 2, size, cols), BF16),
                 pltpu.VMEM((2, parts, size, cols), F32),
                 pltpu.VMEM((2, cols, cols), F32),
-                pltpu.VMEM((2, size, cols), BF16),
                 dma((5,)),
                 dma((4,)),
                 dma((3,)),
                 dma((3,)),
                 dma((chips,)),
-                dma((2, stages)),
-                dma((2, stages)),
-                dma((2, stages)),
-                dma((stages, 2)),
+                dma((stages,)),
+                dma((stages,)),
+                dma((stages,)),
+                dma((stages,)),
                 dma,
             ],
             compiler_params=pltpu.CompilerParams(
-                collective_id=0, has_side_effects=True, vmem_limit_bytes=67043328
+                collective_id=0, has_side_effects=True, vmem_limit_bytes=GRANT
             ),
-        )(x, gain, wq, wf, wi, wg, low, spike.transpose(0, 2, 1), scale)
+        )(
+            *[
+                pltpu.with_memory_space_constraint(v, pltpu.HBM)
+                for v in (x, gain, wq, wf, wi, wg, low, spike.transpose(0, 2, 1), scale)
+            ]
+        )
 
     in_specs = (
         P("pp", "tp"),

time: 49.1 us -> 50 us (1.018)
  Pallas kernels: 47.6 us -> 49.2 us
  local copies, waits for them, and re-layouts: 1.38 us -> 0.62 us
    pallas_call x1, Pallas kernels: 47.6 us -> 49.2 us  [step(): pl.pallas_call(functools.partial(kernel, stages, lanes_axis), out_shape=j...]
    unnamed x1, local copies, waits for them, and re-layouts: 1.38 us -> 0.62 us
where the time goes in v2:
time: 50 us; the launch traced here: 49.9 us
  Pallas kernels  49.2 us (98%)
  local copies, waits for them, and re-layouts  0.62 us (1%)
    pallas_call x1, Pallas kernels, step(): pl.pallas_call(functools.partial(kernel, stages, lanes_axis), out_shape=j...  49.2 us

profile of v2, /device:TPU:3, one launch (start us, length us, event | category | flops | bytes accessed | tf_op | source)
XLA Modules:
  0.0 49.9 jit_solution(13286213995352780306)
XLA Ops:
  0.0 49.2 %shard_map.91 = bf16[64,256]{1,0:T(8,128)(2,1)S(1)} custom-call(bf16[64,256]{1,0:T(8,128)(2,1)} %x_ref.1, f32[1,2048]{1,0:T(1,128)} %gain_ref.1, bf16[1,256,2048]{2,1,0:T(8,128)(2,1)} %wq_ref.1, bf16[1,256,2048]{2,1,0:T(8,128)(2,1)} %wf_ref.1, bf16[1,256,2048]{2,1,0:T(8,128)(2,1)} %wi_ref.1, bf16[1,256,2048]{2,1,0:T(8,128)(2,1)} %wg_ref.1, ...), custom_call_target="tpu_custom_call" | custom-call | tf_op jit(solution)/shard_map/pallas_call | solution.py:475
  49.2 0.6 %copy.11 = bf16[64,256]{1,0:T(8,128)(2,1)} copy(bf16[64,256]{1,0:T(8,128)(2,1)S(1)} %shard_map.91) | data formatting | bytes 65536

commit v3 on v2

--- a/solution.py
+++ b/solution.py
@@ -68,7 +68,7 @@
     rows, cols = xv.shape
     size = buf.shape[4]
     heads = cols // HEAD
-    width = gain_v.shape[1]
+    width = turned.shape[1]
     positions = spike_raw.shape[2]
     parts = positions // size
     spans = positions // rows
@@ -83,26 +83,62 @@
     partner = z * 2 + other
 
     barrier = pltpu.get_barrier_semaphore()
-    for up in range(stages):
+
+    def ready(to_stage, to_lane):
+        pl.semaphore_signal(
+            barrier,
+            inc=1,
+            device_id=at(to_stage, to_lane),
+            device_id_type=pl.DeviceIdType.MESH,
+        )
+
+    ready(stage, partner)
+
+    @pl.when(stage == 0)
+    def _():
+        for source in range(stages):
+            for over in range(chips):
+                ready(source, over * 2 + other)
+
+    @pl.when(stage == 1)
+    def _():
         for over in range(lanes_axis):
-            if up or over:
-                pl.semaphore_signal(
-                    barrier,
-                    inc=1,
-                    device_id=at(
-                        lax.rem(stage + up, stages), lax.rem(lane + over, lanes_axis)
-                    ),
-                    device_id_type=pl.DeviceIdType.MESH,
-                )
+            ready(0, over)
+
+    @pl.when(stage > 1)
+    def _():
+        for over in range(chips):
+            ready(stage - 1, over * 2 + other)
+
+    ready_from_last = [(last, z * 2 + c) for c in range(2)]
+    for c in range(2):
+
+        @pl.when((stage != last) | (core != c))
+        def _():
+            ready(*ready_from_last[c])
+
+    onward = jnp.where(
+        stage == 0,
+        2 * chips,
+        jnp.where(stage == last, 2 * stages - 1, chips),
+    )
+    greetings = 1 + chips + onward
 
     small = [
-        pltpu.make_async_copy(gain_ref, gain_v, load_sem.at[1]),
         pltpu.make_async_copy(scale_ref, scale_v, load_sem.at[2]),
         pltpu.make_async_copy(low_ref, lows.at[core], load_sem.at[3]),
         pltpu.make_async_copy(spike_ref.at[0], spike_raw.at[core], load_sem.at[4]),
     ]
     x_load = pltpu.make_async_copy(x_ref, xv, load_sem.at[0])
     x_load.start()
+    for k in range(chips):
+        small.append(
+            pltpu.make_async_copy(
+                gain_ref.at[:, k * 2 * cols : (k + 1) * 2 * cols],
+                gain_v.at[k],
+                load_sem.at[5 + k],
+            )
+        )
     for load in small:
         load.start()
     loads = []
@@ -133,26 +169,14 @@
             src_ref=xv.at[pl.ds(half * size, size)],
             dst_ref=buf.at[in_slot + half, in_parity, core, z],
             send_sem=in_send.at[target],
-            recv_sem=direct_sem.at[in_slot + half],
-            device_id=at(0, target * 2 + core),
+            recv_sem=direct_sem.at[in_slot + half, in_parity, z],
+            device_id=at(0, target * 2 + other),
             device_id_type=pl.DeviceIdType.MESH,
         )
 
-    def enter():
-        for half in range(2):
-            farthest_first(lambda target: to_first(target, half).start())
-
-            @pl.when(stage != 0)
-            def _():
-                to_first(z, half).start()
-
-            @pl.when(stage == 0)
-            def _():
-                pltpu.make_async_copy(
-                    x_ref.at[pl.ds(half * size, size)],
-                    buf.at[in_slot + half, in_parity, core, z],
-                    direct_sem.at[in_slot + half],
-                ).start()
+    def enter(half):
+        farthest_first(lambda target: to_first(target, half).start())
+        to_first(z, half).start()
 
     def swap_small(which):
         src, dst = (
@@ -201,11 +225,11 @@
             spikes[half, part] = wide
 
     x_load.wait()
-    pl.semaphore_wait(barrier, stages * lanes_axis - 1)
+    pl.semaphore_wait(barrier, greetings)
 
     @pl.when(in_slot == 0)
     def _():
-        enter()
+        enter(0)
 
     for load in small:
         load.wait()
@@ -216,6 +240,11 @@
         swap_small(1).start()
 
     spread(core)
+
+    @pl.when(in_slot == 0)
+    def _():
+        enter(1)
+
     for load in loads:
         load.wait()
 
@@ -236,24 +265,26 @@
 
     @pl.when(in_slot != 0)
     def _():
-        enter()
+        enter(0)
+        enter(1)
 
     def whole_wait(ref, sem):
         pltpu.make_async_copy(ref, ref, sem).wait()
 
-    def gather(slot, parities):
+    def block(slot, parity, k):
         current = jnp.concatenate(
-            [
-                jnp.concatenate(
-                    [buf[slot, parity, k % 2, k // 2] for k in range(lanes_axis)], axis=1
-                )
-                for parity in parities
-            ],
-            axis=0,
+            [buf[slot, parity, c, k] for c in range(2)], axis=1
         ).astype(F32)
         squares = jnp.sum(current * current, axis=1, keepdims=True)
-        scaled = (current * gain_v[...]).astype(BF16)
-        return scaled, lax.rsqrt(squares / width + EPSILON)
+        return (current * gain_v[k]).astype(BF16), squares
+
+    def gather(slot, parity):
+        blocks = [block(slot, parity, k) for k in range(chips)]
+        scaled = jnp.concatenate([b[0] for b in blocks], axis=1)
+        return scaled, inverse_of(sum(b[1] for b in blocks))
+
+    def inverse_of(squares):
+        return lax.rsqrt(squares / width + EPSILON)
 
     out_gain = jnp.concatenate([scale_v[...]] * heads, axis=1)
 
@@ -280,11 +311,11 @@
         )
         scores = jnp.where(tall_mask, mm(tall_query, key_scaled, NT), 0.0).astype(BF16)
         tall_mixed = mm(scores, values, NN)
-        mixed = mm(query_bf, memory.astype(BF16), NT)
-        inner = tall_mixed[0:size]
+        mixed = tall_mixed[0:size]
         for h in range(1, heads):
-            inner = jnp.where(head_of_lane == h, tall_mixed[h * size : (h + 1) * size], inner)
-        mixed = mixed + inner
+            mixed = jnp.where(head_of_lane == h, tall_mixed[h * size : (h + 1) * size], mixed)
+        if memory is not None:
+            mixed = mixed + mm(query_bf, memory.astype(BF16), NT)
         mean_square = mm((mixed * mixed).astype(BF16), mean_ones, NN)
         branch = mixed * lax.rsqrt(mean_square + EPSILON) * out_gain
         branch = branch * (gate_pre * sigmoid(gate_pre))
@@ -293,7 +324,7 @@
     def advance(memory, carried):
         values, key_end, ending = carried
         added = jnp.where(same_head, mm(values, key_end, TN), 0.0)
-        return memory * jnp.exp(ending) + added
+        return added if memory is None else memory * jnp.exp(ending) + added
 
     @pl.when(stage == 0)
     def _():
@@ -302,53 +333,79 @@
                 src_ref=res.at[slot, parity],
                 dst_ref=buf.at[slot, parity, core, z],
                 send_sem=send_sem.at[slot],
-                recv_sem=direct_sem.at[slot],
+                recv_sem=direct_sem.at[slot, parity, z],
                 device_id=at(1, target * 2 + 1 - parity),
                 device_id_type=pl.DeviceIdType.MESH,
             )
 
-        def forward(slot):
-            half = buf.at[slot, :, core]
+        def forward(slot, parity):
+            half = buf.at[slot, parity, other]
             return pltpu.make_async_remote_copy(
                 src_ref=half,
                 dst_ref=half,
-                send_sem=forward_send.at[slot],
-                recv_sem=forward_sem.at[slot],
+                send_sem=forward_send.at[slot, parity],
+                recv_sem=forward_sem.at[slot, parity],
                 device_id=at(stage, partner),
                 device_id_type=pl.DeviceIdType.MESH,
             )
 
-        def pass_on(slot):
-            whole_wait(buf.at[slot, :, core], direct_sem.at[slot])
-            forward(slot).start()
-
-        pass_on(0)
+        def pass_on(slot, parity):
+            for k in range(chips):
+                whole_wait(buf.at[slot, parity, other, k], direct_sem.at[slot, parity, k])
+            forward(slot, parity).start()
+
+        def finish(slot, parity, part, product, inverse, memory):
+            stream = buf[slot, parity, core, z].astype(F32)
+            result, carried = mix(product, inverse, core, part, memory, stream)
+            res[slot, parity] = result
+            farthest_first(lambda target: to_next(slot, parity, target).start())
+            to_next(slot, parity, z).start()
+            state[parity] = advance(memory, carried)
+
+        pass_on(0, 0)
+
+        def single(parity, carry):
+            whole_wait(buf.at[0, parity, core], forward_sem.at[0, parity])
+            scaled, inverse = gather(0, parity)
+            product = mm(scaled, turned[core], NN)
+
+            @pl.when(parity == 0)
+            def _():
+                pass_on(0, 1)
+
+            @pl.when(parity == 1)
+            def _():
+                pass_on(1, 0)
+                pass_on(1, 1)
+
+            finish(0, parity, 0, product, inverse, None)
+            return carry
+
+        lax.fori_loop(0, 2, single, 0)
 
         def step(slot, carry):
             part = lax.rem(slot, parts)
-            whole_wait(buf.at[slot, :, other], forward_sem.at[slot])
-            scaled, inverse = gather(slot, (0, 1))
-            product = mm(scaled, turned[core], NN)
+            for parity in range(2):
+                whole_wait(buf.at[slot, parity, core], forward_sem.at[slot, parity])
+            both = [gather(slot, parity) for parity in range(2)]
+            product = mm(jnp.concatenate([b[0] for b in both], axis=0), turned[core], NN)
 
             @pl.when(slot + 1 < slots)
             def _():
-                pass_on(slot + 1)
+                pass_on(slot + 1, 0)
+                pass_on(slot + 1, 1)
 
             for parity in range(2):
-                own = slice(parity * size, (parity + 1) * size)
                 memory = jnp.where(part == 0, 0.0, state[parity])
-                stream = buf[slot, parity, core, z].astype(F32)
-                result, carried = mix(product[own], inverse[own], core, part, memory, stream)
-                res[slot, parity] = result
-                farthest_first(lambda target: to_next(slot, parity, target).start())
-                to_next(slot, parity, z).start()
-                state[parity] = advance(memory, carried)
+                own = product[parity * size : (parity + 1) * size]
+                finish(slot, parity, part, own, both[parity][1], memory)
             return carry
 
-        lax.fori_loop(0, slots, step, 0)
+        lax.fori_loop(1, slots, step, 0)
 
         def drain(slot, carry):
-            forward(slot).wait_send()
+            for parity in range(2):
+                forward(slot, parity).wait_send()
             whole_wait(buf.at[slot, 0], send_sem.at[slot])
             return carry
 
@@ -363,13 +420,14 @@
         spread(other)
         whole_wait(turned.at[other], swap_recv.at[0])
         parity = lax.rem(core + stage, 2)
+        upper = z // ((chips + 1) // 2)
 
         def to_next(slot, target):
             return pltpu.make_async_remote_copy(
                 src_ref=res.at[slot],
                 dst_ref=buf.at[slot, parity, :, z],
                 send_sem=send_sem.at[slot],
-                recv_sem=direct_sem.at[slot],
+                recv_sem=direct_sem.at[slot, parity, z],
                 device_id=at(lax.rem(stage + 1, stages), target * 2 + other),
                 device_id_type=pl.DeviceIdType.MESH,
             )
@@ -397,11 +455,19 @@
 
         def step(slot, carry):
             part = lax.rem(slot, parts)
-            whole_wait(buf.at[slot, parity], direct_sem.at[slot])
-            scaled, inverse = gather(slot, (parity,))
+            squares, products = 0.0, [0.0, 0.0]
+            for j in range(chips):
+                k = upper * j + (1 - upper) * (chips - 1 - j)
+                whole_wait(buf.at[slot, parity, :, k], direct_sem.at[slot, parity, k])
+                scaled, added = block(slot, parity, k)
+                squares = squares + added
+                span = pl.ds(pl.multiple_of(k * 2 * cols, 2 * cols), 2 * cols)
+                for half in range(2):
+                    products[half] = products[half] + mm(scaled, turned[half, span], NN)
+            inverse = inverse_of(squares)
             kept = []
             for half in range(2):
-                product = mm(scaled, turned[half], NN)
+                product = products[half]
                 memory = jnp.where(part == 0, 0.0, state[half])
                 stream = buf[slot, parity, half, z].astype(F32)
                 result, carried = mix(product, inverse, half, part, memory, stream)
@@ -449,10 +515,7 @@
         swap_small(1).wait_send()
 
     for target in range(chips):
-
-        @pl.when((stage != 0) | (z != target))
-        def _():
-            whole_wait(xv, in_send.at[target])
+        whole_wait(xv, in_send.at[target])
 
     whole_wait(out_ref, out_sem)
 
@@ -479,7 +542,7 @@
             out_specs=vmem,
             scratch_shapes=[
                 pltpu.VMEM((rows, cols), BF16),
-                pltpu.VMEM((1, width), F32),
+                pltpu.VMEM((chips, 1, 2 * cols), F32),
                 pltpu.VMEM(scale.shape, F32),
                 pltpu.VMEM((2, 1, cols), F32),
                 pltpu.VMEM((2, heads, positions), F32),
@@ -489,14 +552,14 @@
                 pltpu.VMEM((stages, 2, size, cols), BF16),
                 pltpu.VMEM((2, parts, size, cols), F32),
                 pltpu.VMEM((2, cols, cols), F32),
-                dma((5,)),
+                dma((5 + chips,)),
                 dma((4,)),
                 dma((3,)),
                 dma((3,)),
                 dma((chips,)),
-                dma((stages,)),
-                dma((stages,)),
-                dma((stages,)),
+                dma((stages, 2, chips)),
+                dma((stages, 2)),
+                dma((stages, 2)),
                 dma((stages,)),
                 dma,
             ],

time: 50 us -> 47.1 us (0.942)
  Pallas kernels: 49.2 us -> 45.9 us
    pallas_call x1, Pallas kernels: 49.2 us -> 45.9 us  [step(): pl.pallas_call(functools.partial(kernel, stages, lanes_axis), out_shape=j...]
where the time goes in v3:
time: 47.1 us; the launch traced here: 46.6 us
  Pallas kernels  45.9 us (97%)
  local copies, waits for them, and re-layouts  0.62 us (1%)
    pallas_call x1, Pallas kernels, step(): pl.pallas_call(functools.partial(kernel, stages, lanes_axis), out_shape=j...  45.9 us

profile of v3, /device:TPU:3, one launch (start us, length us, event | category | flops | bytes accessed | tf_op | source)
XLA Modules:
  0.0 46.6 jit_solution(16146481763923375194)
XLA Ops:
  0.0 45.9 %shard_map.91 = bf16[64,256]{1,0:T(8,128)(2,1)S(1)} custom-call(bf16[64,256]{1,0:T(8,128)(2,1)} %x_ref.1, f32[1,2048]{1,0:T(1,128)} %gain_ref.1, bf16[1,256,2048]{2,1,0:T(8,128)(2,1)} %wq_ref.1, bf16[1,256,2048]{2,1,0:T(8,128)(2,1)} %wf_ref.1, bf16[1,256,2048]{2,1,0:T(8,128)(2,1)} %wi_ref.1, bf16[1,256,2048]{2,1,0:T(8,128)(2,1)} %wg_ref.1, ...), custom_call_target="tpu_custom_call" | custom-call | tf_op jit(solution)/shard_map/pallas_call | solution.py:538
  46.0 0.6 %copy.11 = bf16[64,256]{1,0:T(8,128)(2,1)} copy(bf16[64,256]{1,0:T(8,128)(2,1)S(1)} %shard_map.91) | data formatting | bytes 65536

commit v4 on v3

--- a/solution.py
+++ b/solution.py
@@ -11,6 +11,7 @@
 TILE = 256
 EPSILON = 1e-06
 GRANT = 40 * 2**20
+SENT_AFTER = (1, 4)
 F32 = jnp.float32
 BF16 = jnp.bfloat16
 NT = (((1,), (1,)), ((), ()))
@@ -70,6 +71,7 @@
     heads = cols // HEAD
     width = turned.shape[1]
     positions = spike_raw.shape[2]
+    tiles = width // TILE
     parts = positions // size
     spans = positions // rows
     chips = lanes_axis // 2
@@ -188,7 +190,7 @@
             src_ref=src,
             dst_ref=dst,
             send_sem=swap_send.at[1 + which],
-            recv_sem=swap_recv.at[1 + which],
+            recv_sem=swap_recv.at[tiles + which],
             device_id=at(stage, partner),
             device_id_type=pl.DeviceIdType.MESH,
         )
@@ -199,15 +201,13 @@
             src_ref=tile,
             dst_ref=tile,
             send_sem=swap_send.at[0],
-            recv_sem=swap_recv.at[0],
+            recv_sem=swap_recv.at[k],
             device_id=at(stage, partner),
             device_id_type=pl.DeviceIdType.MESH,
         )
 
     head_of_lane = lax.broadcasted_iota(jnp.int32, (size, cols), 1) // HEAD
-    tri_row = lax.broadcasted_iota(jnp.int32, (size, size), 0)
-    tri_col = lax.broadcasted_iota(jnp.int32, (size, size), 1)
-    tril_ones = jnp.where(tri_row >= tri_col, 1.0, 0.0).astype(BF16)
+    row = lax.broadcasted_iota(jnp.int32, (size, cols), 0)
     tall_row = lax.rem(lax.broadcasted_iota(jnp.int32, (heads * size, size), 0), size)
     tall_col = lax.broadcasted_iota(jnp.int32, (heads * size, size), 1)
     tall_mask = tall_row >= tall_col
@@ -222,7 +222,7 @@
             wide = jnp.zeros((size, cols), F32)
             for h in range(heads):
                 wide = jnp.where(head_of_lane == h, piece[:, h : h + 1], wide)
-            spikes[half, part] = wide
+            spikes[half, part] = jnp.exp(wide)
 
     x_load.wait()
     pl.semaphore_wait(barrier, greetings)
@@ -240,11 +240,6 @@
         swap_small(1).start()
 
     spread(core)
-
-    @pl.when(in_slot == 0)
-    def _():
-        enter(1)
-
     for load in loads:
         load.wait()
 
@@ -263,9 +258,8 @@
 
     lax.fori_loop(0, width // TILE, turn, 0)
 
-    @pl.when(in_slot != 0)
-    def _():
-        enter(0)
+    @pl.when(in_slot == 0)
+    def _():
         enter(1)
 
     def whole_wait(ref, sem):
@@ -296,14 +290,16 @@
         gate_pre = projected[:, 3 * cols : 4 * cols]
 
         key_in = (1.0 - lows[half]) * sigmoid(-forget_pre)
-        log_forget = jnp.log(1.0 - key_in) + spikes[half, part]
-        high = log_forget.astype(BF16)
-        low = (log_forget - high.astype(F32)).astype(BF16)
-        running = mm(tril_ones, high, NN) + mm(tril_ones, low, NN)
-        ending = running[size - 1 : size, :]
-        query_scaled = query_pre * sigmoid(query_pre) * jnp.exp(running)
-        key_scaled = (key_in * jnp.exp(-running)).astype(BF16)
-        key_end = (key_in * jnp.exp(ending - running)).astype(BF16)
+        decay = (1.0 - key_in) * spikes[half, part]
+        reach = 1
+        while reach < size:
+            decay = decay * jnp.where(row < reach, 1.0, pltpu.roll(decay, reach, 0))
+            reach *= 2
+        ending = decay[size - 1 : size, :]
+        query_scaled = query_pre * sigmoid(query_pre) * decay
+        key_grown = key_in / decay
+        key_scaled = key_grown.astype(BF16)
+        key_end = (key_grown * ending).astype(BF16)
         query_bf = query_scaled.astype(BF16)
         tall_query = jnp.concatenate(
             [jnp.where(head_of_lane == h, query_scaled, 0.0).astype(BF16) for h in range(heads)],
@@ -324,7 +320,7 @@
     def advance(memory, carried):
         values, key_end, ending = carried
         added = jnp.where(same_head, mm(values, key_end, TN), 0.0)
-        return added if memory is None else memory * jnp.exp(ending) + added
+        return added if memory is None else memory * ending + added
 
     @pl.when(stage == 0)
     def _():
@@ -413,12 +409,19 @@
 
     @pl.when(stage != 0)
     def _():
-        tiles = width // TILE
         swap_tile(tiles - 1).start()
         swap_small(0).wait_recv()
         swap_small(1).wait_recv()
         spread(other)
-        whole_wait(turned.at[other], swap_recv.at[0])
+        for k in range(tiles):
+            whole_wait(turned.at[other, pl.ds(k * TILE, TILE)], swap_recv.at[k])
+            for half in range(2):
+                if k == SENT_AFTER[half]:
+
+                    @pl.when(in_slot != 0)
+                    def _():
+                        enter(half)
+
         parity = lax.rem(core + stage, 2)
         upper = z // ((chips + 1) // 2)
 
@@ -555,7 +558,7 @@
                 dma((5 + chips,)),
                 dma((4,)),
                 dma((3,)),
-                dma((3,)),
+                dma((width // TILE + 2,)),
                 dma((chips,)),
                 dma((stages, 2, chips)),
                 dma((stages, 2)),

time: 47.1 us -> 44.6 us (0.947)
  Pallas kernels: 45.9 us -> 43.5 us
    pallas_call x1, Pallas kernels: 45.9 us -> 43.5 us  [step(): pl.pallas_call(functools.partial(kernel, stages, lanes_axis), out_shape=j...]
where the time goes in v4:
time: 44.6 us; the launch traced here: 44.1 us
  Pallas kernels  43.5 us (98%)
  local copies, waits for them, and re-layouts  0.62 us (1%)
    pallas_call x1, Pallas kernels, step(): pl.pallas_call(functools.partial(kernel, stages, lanes_axis), out_shape=j...  43.5 us

profile of v4, /device:TPU:3, one launch (start us, length us, event | category | flops | bytes accessed | tf_op | source)
XLA Modules:
  0.0 44.1 jit_solution(2007909465715147042)
XLA Ops:
  0.0 43.5 %shard_map.91 = bf16[64,256]{1,0:T(8,128)(2,1)S(1)} custom-call(bf16[64,256]{1,0:T(8,128)(2,1)} %x_ref.1, f32[1,2048]{1,0:T(1,128)} %gain_ref.1, bf16[1,256,2048]{2,1,0:T(8,128)(2,1)} %wq_ref.1, bf16[1,256,2048]{2,1,0:T(8,128)(2,1)} %wf_ref.1, bf16[1,256,2048]{2,1,0:T(8,128)(2,1)} %wi_ref.1, bf16[1,256,2048]{2,1,0:T(8,128)(2,1)} %wg_ref.1, ...), custom_call_target="tpu_custom_call" | custom-call | tf_op jit(solution)/shard_map/pallas_call | solution.py:541
  43.5 0.6 %copy.11 = bf16[64,256]{1,0:T(8,128)(2,1)} copy(bf16[64,256]{1,0:T(8,128)(2,1)S(1)} %shard_map.91) | data formatting | bytes 65536

commit v5 on v4

--- a/solution.py
+++ b/solution.py
@@ -166,6 +166,10 @@
             def _():
                 send(z - far)
 
+    def own_first(send):
+        send(z)
+        farthest_first(send)
+
     def to_first(target, half):
         return pltpu.make_async_remote_copy(
             src_ref=xv.at[pl.ds(half * size, size)],
@@ -214,6 +218,7 @@
     sq_row = lax.broadcasted_iota(jnp.int32, (cols, cols), 0) // HEAD
     sq_col = lax.broadcasted_iota(jnp.int32, (cols, cols), 1) // HEAD
     same_head = sq_row == sq_col
+    lane_head = lax.broadcasted_iota(jnp.int32, (HEAD, cols), 1) // HEAD
     mean_ones = jnp.where(same_head, 1.0 / HEAD, 0.0).astype(BF16)
 
     def spread(half):
@@ -311,7 +316,8 @@
         for h in range(1, heads):
             mixed = jnp.where(head_of_lane == h, tall_mixed[h * size : (h + 1) * size], mixed)
         if memory is not None:
-            mixed = mixed + mm(query_bf, memory.astype(BF16), NT)
+            tiled = jnp.concatenate([memory.astype(BF16)] * heads, axis=0)
+            mixed = mixed + mm(query_bf, jnp.where(same_head, tiled, jnp.zeros_like(tiled)), NT)
         mean_square = mm((mixed * mixed).astype(BF16), mean_ones, NN)
         branch = mixed * lax.rsqrt(mean_square + EPSILON) * out_gain
         branch = branch * (gate_pre * sigmoid(gate_pre))
@@ -319,7 +325,10 @@
 
     def advance(memory, carried):
         values, key_end, ending = carried
-        added = jnp.where(same_head, mm(values, key_end, TN), 0.0)
+        spread_out = mm(values, key_end, TN)
+        added = spread_out[0:HEAD]
+        for h in range(1, heads):
+            added = jnp.where(lane_head == h, spread_out[h * HEAD : (h + 1) * HEAD], added)
         return added if memory is None else memory * ending + added
 
     @pl.when(stage == 0)
@@ -328,7 +337,7 @@
             return pltpu.make_async_remote_copy(
                 src_ref=res.at[slot, parity],
                 dst_ref=buf.at[slot, parity, core, z],
-                send_sem=send_sem.at[slot],
+                send_sem=send_sem.at[slot, parity],
                 recv_sem=direct_sem.at[slot, parity, z],
                 device_id=at(1, target * 2 + 1 - parity),
                 device_id_type=pl.DeviceIdType.MESH,
@@ -350,12 +359,21 @@
                 whole_wait(buf.at[slot, parity, other, k], direct_sem.at[slot, parity, k])
             forward(slot, parity).start()
 
+        def sent(slot):
+            for parity in range(2):
+                whole_wait(buf.at[slot, parity, core], send_sem.at[slot, parity])
+
+        def turn_of(slot, parity):
+            @pl.when((slot > 0) & (parity == 0))
+            def _():
+                sent(slot - 1)
+
         def finish(slot, parity, part, product, inverse, memory):
             stream = buf[slot, parity, core, z].astype(F32)
             result, carried = mix(product, inverse, core, part, memory, stream)
             res[slot, parity] = result
-            farthest_first(lambda target: to_next(slot, parity, target).start())
-            to_next(slot, parity, z).start()
+            turn_of(slot, parity)
+            own_first(lambda target: to_next(slot, parity, target).start())
             state[parity] = advance(memory, carried)
 
         pass_on(0, 0)
@@ -402,10 +420,10 @@
         def drain(slot, carry):
             for parity in range(2):
                 forward(slot, parity).wait_send()
-            whole_wait(buf.at[slot, 0], send_sem.at[slot])
             return carry
 
         lax.fori_loop(0, slots, drain, 0)
+        sent(slots - 1)
 
     @pl.when(stage != 0)
     def _():
@@ -429,7 +447,7 @@
             return pltpu.make_async_remote_copy(
                 src_ref=res.at[slot],
                 dst_ref=buf.at[slot, parity, :, z],
-                send_sem=send_sem.at[slot],
+                send_sem=send_sem.at[slot, 0],
                 recv_sem=direct_sem.at[slot, parity, z],
                 device_id=at(lax.rem(stage + 1, stages), target * 2 + other),
                 device_id_type=pl.DeviceIdType.MESH,
@@ -447,7 +465,7 @@
             return pltpu.make_async_remote_copy(
                 src_ref=res.at[slot, half],
                 dst_ref=place(slot),
-                send_sem=send_sem.at[slot],
+                send_sem=send_sem.at[slot, half],
                 recv_sem=out_sem,
                 device_id=at(owner(slot), z * 2 + half),
                 device_id_type=pl.DeviceIdType.MESH,
@@ -479,8 +497,7 @@
 
             @pl.when(stage != last)
             def _():
-                farthest_first(lambda target: to_next(slot, target).start())
-                to_next(slot, z).start()
+                own_first(lambda target: to_next(slot, target).start())
 
             for half in range(2):
 
@@ -502,7 +519,7 @@
         def drain(slot, carry):
             @pl.when(stage != last)
             def _():
-                whole_wait(buf.at[slot, 0], send_sem.at[slot])
+                whole_wait(buf.at[slot, 0], send_sem.at[slot, 0])
 
             for half in range(2):
 
@@ -554,7 +571,7 @@
                 pltpu.VMEM((stages, 2, 2, chips, size, cols), BF16),
                 pltpu.VMEM((stages, 2, size, cols), BF16),
                 pltpu.VMEM((2, parts, size, cols), F32),
-                pltpu.VMEM((2, cols, cols), F32),
+                pltpu.VMEM((2, HEAD, cols), F32),
                 dma((5 + chips,)),
                 dma((4,)),
                 dma((3,)),
@@ -563,7 +580,7 @@
                 dma((stages, 2, chips)),
                 dma((stages, 2)),
                 dma((stages, 2)),
-                dma((stages,)),
+                dma((stages, 2)),
                 dma,
             ],
             compiler_params=pltpu.CompilerParams(

time: 44.6 us -> 44.4 us (level)
  no operation moved by 1% of the time
where the time goes in v5:
time: 44.4 us; the launch traced here: 43.8 us
  Pallas kernels  43.2 us (97%)
  local copies, waits for them, and re-layouts  0.62 us (1%)
    pallas_call x1, Pallas kernels, step(): pl.pallas_call(functools.partial(kernel, stages, lanes_axis), out_shape=j...  43.2 us

profile of v5, /device:TPU:3, one launch (start us, length us, event | category | flops | bytes accessed | tf_op | source)
XLA Modules:
  0.0 43.8 jit_solution(14405756167847887172)
XLA Ops:
  0.0 43.2 %shard_map.91 = bf16[64,256]{1,0:T(8,128)(2,1)S(1)} custom-call(bf16[64,256]{1,0:T(8,128)(2,1)} %x_ref.1, f32[1,2048]{1,0:T(1,128)} %gain_ref.1, bf16[1,256,2048]{2,1,0:T(8,128)(2,1)} %wq_ref.1, bf16[1,256,2048]{2,1,0:T(8,128)(2,1)} %wf_ref.1, bf16[1,256,2048]{2,1,0:T(8,128)(2,1)} %wi_ref.1, bf16[1,256,2048]{2,1,0:T(8,128)(2,1)} %wg_ref.1, ...), custom_call_target="tpu_custom_call" | custom-call | tf_op jit(solution)/shard_map/pallas_call | solution.py:558
  43.2 0.6 %copy.11 = bf16[64,256]{1,0:T(8,128)(2,1)} copy(bf16[64,256]{1,0:T(8,128)(2,1)S(1)} %shard_map.91) | data formatting | bytes 65536

commit v6 on v5

--- a/solution.py
+++ b/solution.py
@@ -11,7 +11,6 @@
 TILE = 256
 EPSILON = 1e-06
 GRANT = 40 * 2**20
-SENT_AFTER = (1, 4)
 F32 = jnp.float32
 BF16 = jnp.bfloat16
 NT = (((1,), (1,)), ((), ()))
@@ -72,6 +71,7 @@
     width = turned.shape[1]
     positions = spike_raw.shape[2]
     tiles = width // TILE
+    groups = tiles // 3 + 1
     parts = positions // size
     spans = positions // rows
     chips = lanes_axis // 2
@@ -134,26 +134,22 @@
     x_load = pltpu.make_async_copy(x_ref, xv, load_sem.at[0])
     x_load.start()
     for k in range(chips):
-        small.append(
-            pltpu.make_async_copy(
-                gain_ref.at[:, k * 2 * cols : (k + 1) * 2 * cols],
-                gain_v.at[k],
-                load_sem.at[5 + k],
-            )
-        )
+        pltpu.make_async_copy(
+            gain_ref.at[:, k * 2 * cols : (k + 1) * 2 * cols], gain_v.at[k], load_sem.at[1]
+        ).start()
     for load in small:
         load.start()
-    loads = []
     for role, ref in enumerate((wq_ref, wf_ref, wi_ref, wg_ref)):
-        load = pltpu.make_async_copy(
-            ref.at[0], weights.at[pl.ds(role * cols, cols)], w_sem.at[role]
-        )
-        load.start()
-        loads.append(load)
+        pltpu.make_async_copy(
+            ref.at[0], weights.at[pl.ds(role * cols, cols)], w_sem
+        ).start()
 
     sequence = stage // spans
     in_parity = lax.rem(sequence, 2)
     in_slot = (sequence // 2) * parts + lax.rem(stage, spans) * 2
+
+    def whole_wait(ref, sem):
+        pltpu.make_async_copy(ref, ref, sem).wait()
 
     def farthest_first(send):
         for far in range(chips - 1, 0, -1):
@@ -174,8 +170,8 @@
         return pltpu.make_async_remote_copy(
             src_ref=xv.at[pl.ds(half * size, size)],
             dst_ref=buf.at[in_slot + half, in_parity, core, z],
-            send_sem=in_send.at[target],
-            recv_sem=direct_sem.at[in_slot + half, in_parity, z],
+            send_sem=in_send,
+            recv_sem=direct_sem.at[in_slot + half, in_parity],
             device_id=at(0, target * 2 + other),
             device_id_type=pl.DeviceIdType.MESH,
         )
@@ -194,7 +190,7 @@
             src_ref=src,
             dst_ref=dst,
             send_sem=swap_send.at[1 + which],
-            recv_sem=swap_recv.at[tiles + which],
+            recv_sem=swap_recv.at[groups + which],
             device_id=at(stage, partner),
             device_id_type=pl.DeviceIdType.MESH,
         )
@@ -205,7 +201,7 @@
             src_ref=tile,
             dst_ref=tile,
             send_sem=swap_send.at[0],
-            recv_sem=swap_recv.at[k],
+            recv_sem=swap_recv.at[(k + 1) // 3],
             device_id=at(stage, partner),
             device_id_type=pl.DeviceIdType.MESH,
         )
@@ -238,6 +234,7 @@
 
     for load in small:
         load.wait()
+    whole_wait(gain_v, load_sem.at[1])
 
     @pl.when(stage != 0)
     def _():
@@ -245,8 +242,7 @@
         swap_small(1).start()
 
     spread(core)
-    for load in loads:
-        load.wait()
+    whole_wait(weights, w_sem)
 
     def turn(k, carry):
         tile = pl.ds(pl.multiple_of(k * TILE, TILE), TILE)
@@ -266,9 +262,6 @@
     @pl.when(in_slot == 0)
     def _():
         enter(1)
-
-    def whole_wait(ref, sem):
-        pltpu.make_async_copy(ref, ref, sem).wait()
 
     def block(slot, parity, k):
         current = jnp.concatenate(
@@ -338,7 +331,7 @@
                 src_ref=res.at[slot, parity],
                 dst_ref=buf.at[slot, parity, core, z],
                 send_sem=send_sem.at[slot, parity],
-                recv_sem=direct_sem.at[slot, parity, z],
+                recv_sem=direct_sem.at[slot, z],
                 device_id=at(1, target * 2 + 1 - parity),
                 device_id_type=pl.DeviceIdType.MESH,
             )
@@ -348,15 +341,14 @@
             return pltpu.make_async_remote_copy(
                 src_ref=half,
                 dst_ref=half,
-                send_sem=forward_send.at[slot, parity],
+                send_sem=forward_send,
                 recv_sem=forward_sem.at[slot, parity],
                 device_id=at(stage, partner),
                 device_id_type=pl.DeviceIdType.MESH,
             )
 
         def pass_on(slot, parity):
-            for k in range(chips):
-                whole_wait(buf.at[slot, parity, other, k], direct_sem.at[slot, parity, k])
+            whole_wait(buf.at[slot, parity, other], direct_sem.at[slot, parity])
             forward(slot, parity).start()
 
         def sent(slot):
@@ -417,12 +409,7 @@
 
         lax.fori_loop(1, slots, step, 0)
 
-        def drain(slot, carry):
-            for parity in range(2):
-                forward(slot, parity).wait_send()
-            return carry
-
-        lax.fori_loop(0, slots, drain, 0)
+        whole_wait(buf.at[:, :, 0], forward_send)
         sent(slots - 1)
 
     @pl.when(stage != 0)
@@ -431,14 +418,15 @@
         swap_small(0).wait_recv()
         swap_small(1).wait_recv()
         spread(other)
-        for k in range(tiles):
-            whole_wait(turned.at[other, pl.ds(k * TILE, TILE)], swap_recv.at[k])
-            for half in range(2):
-                if k == SENT_AFTER[half]:
-
-                    @pl.when(in_slot != 0)
-                    def _():
-                        enter(half)
+        for group in range(groups):
+            first, end = max(group * 3 - 1, 0), min(group * 3 + 2, tiles)
+            lines = pl.ds(first * TILE, (end - first) * TILE)
+            whole_wait(turned.at[other, lines], swap_recv.at[group])
+            if group < 2:
+
+                @pl.when(in_slot != 0)
+                def _():
+                    enter(group)
 
         parity = lax.rem(core + stage, 2)
         upper = z // ((chips + 1) // 2)
@@ -448,7 +436,7 @@
                 src_ref=res.at[slot],
                 dst_ref=buf.at[slot, parity, :, z],
                 send_sem=send_sem.at[slot, 0],
-                recv_sem=direct_sem.at[slot, parity, z],
+                recv_sem=direct_sem.at[slot, z],
                 device_id=at(lax.rem(stage + 1, stages), target * 2 + other),
                 device_id_type=pl.DeviceIdType.MESH,
             )
@@ -479,7 +467,7 @@
             squares, products = 0.0, [0.0, 0.0]
             for j in range(chips):
                 k = upper * j + (1 - upper) * (chips - 1 - j)
-                whole_wait(buf.at[slot, parity, :, k], direct_sem.at[slot, parity, k])
+                whole_wait(buf.at[slot, parity, :, k], direct_sem.at[slot, k])
                 scaled, added = block(slot, parity, k)
                 squares = squares + added
                 span = pl.ds(pl.multiple_of(k * 2 * cols, 2 * cols), 2 * cols)
@@ -534,8 +522,7 @@
         swap_small(0).wait_send()
         swap_small(1).wait_send()
 
-    for target in range(chips):
-        whole_wait(xv, in_send.at[target])
+    whole_wait(buf.at[0, 0], in_send)
 
     whole_wait(out_ref, out_sem)
 
@@ -572,14 +559,14 @@
                 pltpu.VMEM((stages, 2, size, cols), BF16),
                 pltpu.VMEM((2, parts, size, cols), F32),
                 pltpu.VMEM((2, HEAD, cols), F32),
-                dma((5 + chips,)),
-                dma((4,)),
+                dma((5,)),
+                dma,
                 dma((3,)),
-                dma((width // TILE + 2,)),
-                dma((chips,)),
-                dma((stages, 2, chips)),
+                dma((width // TILE // 3 + 3,)),
+                dma,
+                dma((stages, chips)),
                 dma((stages, 2)),
-                dma((stages, 2)),
+                dma,
                 dma((stages, 2)),
                 dma,
             ],

time: 44.4 us -> 44.1 us (level)
  no operation moved by 1% of the time
where the time goes in v6:
time: 44.1 us; the launch traced here: 43.4 us
  Pallas kernels  42.8 us (97%)
  local copies, waits for them, and re-layouts  0.62 us (1%)
    pallas_call x1, Pallas kernels, step(): pl.pallas_call(functools.partial(kernel, stages, lanes_axis), out_shape=j...  42.8 us

profile of v6, /device:TPU:3, one launch (start us, length us, event | category | flops | bytes accessed | tf_op | source)
XLA Modules:
  0.0 43.4 jit_solution(16835770165924637699)
XLA Ops:
  0.0 42.8 %shard_map.91 = bf16[64,256]{1,0:T(8,128)(2,1)S(1)} custom-call(bf16[64,256]{1,0:T(8,128)(2,1)} %x_ref.1, f32[1,2048]{1,0:T(1,128)} %gain_ref.1, bf16[1,256,2048]{2,1,0:T(8,128)(2,1)} %wq_ref.1, bf16[1,256,2048]{2,1,0:T(8,128)(2,1)} %wf_ref.1, bf16[1,256,2048]{2,1,0:T(8,128)(2,1)} %wi_ref.1, bf16[1,256,2048]{2,1,0:T(8,128)(2,1)} %wg_ref.1, ...), custom_call_target="tpu_custom_call" | custom-call | tf_op jit(solution)/shard_map/pallas_call | solution.py:545
  42.8 0.6 %copy.11 = bf16[64,256]{1,0:T(8,128)(2,1)} copy(bf16[64,256]{1,0:T(8,128)(2,1)S(1)} %shard_map.91) | data formatting | bytes 65536

commit v7 on v6

--- a/solution.py
+++ b/solution.py
@@ -331,7 +331,7 @@
                 src_ref=res.at[slot, parity],
                 dst_ref=buf.at[slot, parity, core, z],
                 send_sem=send_sem.at[slot, parity],
-                recv_sem=direct_sem.at[slot, z],
+                recv_sem=direct_sem.at[slot, 0],
                 device_id=at(1, target * 2 + 1 - parity),
                 device_id_type=pl.DeviceIdType.MESH,
             )
@@ -351,14 +351,14 @@
             whole_wait(buf.at[slot, parity, other], direct_sem.at[slot, parity])
             forward(slot, parity).start()
 
-        def sent(slot):
-            for parity in range(2):
-                whole_wait(buf.at[slot, parity, core], send_sem.at[slot, parity])
+        def sent(slot, parity):
+            whole_wait(buf.at[slot, parity, core], send_sem.at[slot, parity])
 
         def turn_of(slot, parity):
-            @pl.when((slot > 0) & (parity == 0))
-            def _():
-                sent(slot - 1)
+            @pl.when(slot * 2 + parity > 0)
+            def _():
+                before = slot * 2 + parity - 1
+                sent(before // 2, lax.rem(before, 2))
 
         def finish(slot, parity, part, product, inverse, memory):
             stream = buf[slot, parity, core, z].astype(F32)
@@ -410,7 +410,7 @@
         lax.fori_loop(1, slots, step, 0)
 
         whole_wait(buf.at[:, :, 0], forward_send)
-        sent(slots - 1)
+        sent(slots - 1, 1)
 
     @pl.when(stage != 0)
     def _():
@@ -429,14 +429,13 @@
                     enter(group)
 
         parity = lax.rem(core + stage, 2)
-        upper = z // ((chips + 1) // 2)
 
         def to_next(slot, target):
             return pltpu.make_async_remote_copy(
                 src_ref=res.at[slot],
                 dst_ref=buf.at[slot, parity, :, z],
                 send_sem=send_sem.at[slot, 0],
-                recv_sem=direct_sem.at[slot, z],
+                recv_sem=direct_sem.at[slot, 0],
                 device_id=at(lax.rem(stage + 1, stages), target * 2 + other),
                 device_id_type=pl.DeviceIdType.MESH,
             )
@@ -464,16 +463,9 @@
 
         def step(slot, carry):
             part = lax.rem(slot, parts)
-            squares, products = 0.0, [0.0, 0.0]
-            for j in range(chips):
-                k = upper * j + (1 - upper) * (chips - 1 - j)
-                whole_wait(buf.at[slot, parity, :, k], direct_sem.at[slot, k])
-                scaled, added = block(slot, parity, k)
-                squares = squares + added
-                span = pl.ds(pl.multiple_of(k * 2 * cols, 2 * cols), 2 * cols)
-                for half in range(2):
-                    products[half] = products[half] + mm(scaled, turned[half, span], NN)
-            inverse = inverse_of(squares)
+            whole_wait(buf.at[slot, parity], direct_sem.at[slot, 0])
+            scaled, inverse = gather(slot, parity)
+            products = [mm(scaled, turned[half], NN) for half in range(2)]
             kept = []
             for half in range(2):
                 product = products[half]
@@ -564,7 +556,7 @@
                 dma((3,)),
                 dma((width // TILE // 3 + 3,)),
                 dma,
-                dma((stages, chips)),
+                dma((stages, 2)),
                 dma((stages, 2)),
                 dma,
                 dma((stages, 2)),

time: 44.1 us -> 43.8 us (level)
  no operation moved by 1% of the time
where the time goes in v7:
time: 43.8 us; the launch traced here: 43.4 us
  Pallas kernels  42.8 us (98%)
  local copies, waits for them, and re-layouts  0.62 us (1%)
    pallas_call x1, Pallas kernels, step(): pl.pallas_call(functools.partial(kernel, stages, lanes_axis), out_shape=j...  42.8 us

profile of v7, /device:TPU:3, one launch (start us, length us, event | category | flops | bytes accessed | tf_op | source)
XLA Modules:
  0.0 43.4 jit_solution(2405782370439004875)
XLA Ops:
  0.0 42.8 %shard_map.91 = bf16[64,256]{1,0:T(8,128)(2,1)S(1)} custom-call(bf16[64,256]{1,0:T(8,128)(2,1)} %x_ref.1, f32[1,2048]{1,0:T(1,128)} %gain_ref.1, bf16[1,256,2048]{2,1,0:T(8,128)(2,1)} %wq_ref.1, bf16[1,256,2048]{2,1,0:T(8,128)(2,1)} %wf_ref.1, bf16[1,256,2048]{2,1,0:T(8,128)(2,1)} %wi_ref.1, bf16[1,256,2048]{2,1,0:T(8,128)(2,1)} %wg_ref.1, ...), custom_call_target="tpu_custom_call" | custom-call | tf_op jit(solution)/shard_map/pallas_call | solution.py:537
  42.8 0.6 %copy.11 = bf16[64,256]{1,0:T(8,128)(2,1)} copy(bf16[64,256]{1,0:T(8,128)(2,1)S(1)} %shard_map.91) | data formatting | bytes 65536

commit v8 on v7

--- a/solution.py
+++ b/solution.py
@@ -139,7 +139,7 @@
         ).start()
     for load in small:
         load.start()
-    for role, ref in enumerate((wq_ref, wf_ref, wi_ref, wg_ref)):
+    for role, ref in enumerate((wf_ref, wq_ref, wi_ref, wg_ref)):
         pltpu.make_async_copy(
             ref.at[0], weights.at[pl.ds(role * cols, cols)], w_sem
         ).start()
@@ -282,8 +282,8 @@
 
     def mix(product, inverse, half, part, memory, stream):
         projected = product * inverse
-        query_pre = projected[:, 0 * cols : 1 * cols]
-        forget_pre = projected[:, 1 * cols : 2 * cols]
+        forget_pre = projected[:, 0 * cols : 1 * cols]
+        query_pre = projected[:, 1 * cols : 2 * cols]
         values = projected[:, 2 * cols : 3 * cols].astype(BF16)
         gate_pre = projected[:, 3 * cols : 4 * cols]
 

time: 43.8 us -> 43.8 us (level)
  no operation moved by 1% of the time
where the time goes in v8:
time: 43.8 us; the launch traced here: 43.4 us
  Pallas kernels  42.8 us (98%)
  local copies, waits for them, and re-layouts  0.62 us (1%)
    pallas_call x1, Pallas kernels, step(): pl.pallas_call(functools.partial(kernel, stages, lanes_axis), out_shape=j...  42.8 us

profile of v8, /device:TPU:3, one launch (start us, length us, event | category | flops | bytes accessed | tf_op | source)
XLA Modules:
  0.0 43.4 jit_solution(16463775981595788521)
XLA Ops:
  0.0 42.8 %shard_map.91 = bf16[64,256]{1,0:T(8,128)(2,1)S(1)} custom-call(bf16[64,256]{1,0:T(8,128)(2,1)} %x_ref.1, f32[1,2048]{1,0:T(1,128)} %gain_ref.1, bf16[1,256,2048]{2,1,0:T(8,128)(2,1)} %wq_ref.1, bf16[1,256,2048]{2,1,0:T(8,128)(2,1)} %wf_ref.1, bf16[1,256,2048]{2,1,0:T(8,128)(2,1)} %wi_ref.1, bf16[1,256,2048]{2,1,0:T(8,128)(2,1)} %wg_ref.1, ...), custom_call_target="tpu_custom_call" | custom-call | tf_op jit(solution)/shard_map/pallas_call | solution.py:537
  42.8 0.6 %copy.11 = bf16[64,256]{1,0:T(8,128)(2,1)} copy(bf16[64,256]{1,0:T(8,128)(2,1)S(1)} %shard_map.91) | data formatting | bytes 65536
